TPU v7x, 512 devices: a whole 4x4x16 slice. The times are simulated.
512 devices in a mesh: sp: 64 (over z, y), tp: 8 (over x, core).
Axes of the slice: x: 4, y: 4, z: 16, core: 2. Of those that a mesh axis runs over, the one named last changes fastest.
Arguments:
- layer_input_sequence: bfloat16 [24576, 2048], P('sp', 'tp'), may hold values from -6 to 6
- probe_projection_matrix: bfloat16 [2048, 1024], P(None, 'tp'), may hold values from -0.125 to 0.125
- address_projection_matrix: bfloat16 [2048, 1024], P(None, 'tp'), may hold values from -0.125 to 0.125
- content_projection_matrix: bfloat16 [2048, 1024], P(None, 'tp'), may hold values from -2 to 2
- result_valve_matrix: bfloat16 [2048, 1024], P(None, 'tp'), may hold values from -0.125 to 0.125
- shrink_strength_matrix: bfloat16 [2, 2048, 8], replicated, may hold values from -0.125 to 0.125
- causal_filter_coefficients: bfloat16 [3, 4, 1024], P(None, None, 'tp'), may hold values from -3 to 3
- channel_group_fading_speed: float32 [8], replicated, may hold values from 0 to 0.06, as said below
- summed_shrink_logs: float32 [24576, 8], P('sp', 'tp'), may hold values from -0.7 to 0, as said below
- result_scaling_vector: bfloat16 [128], replicated, may hold values from 0.099609375 to 1.8984375
- generated_probe_vector: bfloat16 [64, 8, 128], P('sp', 'tp'), may hold values from -6 to 6
Outputs:
- mixed: bfloat16 [24576, 1024], P('sp', 'tp')
- cache: bfloat16 [8, 128, 128], P('tp')
- new_read: float32 [64, 8, 128], P('sp', 'tp')
Inputs may be any that keep to these rules, and one draw needn't show every extreme that they name: `channel_group_fading_speed`: positive rates of each head. `summed_shrink_logs`: zero at all but a few positions of each head.
All inputs are finite; a program needn't handle non-finite values.
Results may differ from a plain program's by a relative error of at most 0.0095.
Values may be sent and summed in bfloat16 or wider, within the bound.
A program may use at most 64 MiB of HBM per device.

v0:
```python
import math
import jax
import jax.numpy as jnp
from jax import lax
from jax.sharding import PartitionSpec as P

DK = 128
BLK = 64
CONV = 4
EPS = 1e-06
HIGH = lax.Precision.HIGHEST


def sent_to_all(shard, axis):
    count = lax.axis_size(axis)
    return lax.all_to_all(
        jnp.broadcast_to(shard[None], (count, *shard.shape)), axis, 0, 0, tiled=True
    )


def in_order(pieces, dim):
    dims = list(pieces.shape[1:])
    dims[dim] *= pieces.shape[0]
    return jnp.moveaxis(pieces, 0, dim).reshape(dims)


def gathered_copies(shard, axis, dim):
    pieces = sent_to_all(shard, axis)
    return in_order(pieces, dim)


def shifted(block, axis, distance):
    devices = range(lax.axis_size(axis))
    route = [(i - distance, i) for i in devices if i - distance in devices]
    return lax.ppermute(block, axis, route)


def silu(value):
    return value * jax.nn.sigmoid(value)


def l2_unit(value):
    return value * lax.rsqrt(jnp.sum(value * value, axis=-1, keepdims=True) + EPS)


def block_terms(query, keys, values, fading_exponent, beta):
    heads, length, width = keys.shape
    count = length // BLK

    def split(array):
        return array.reshape((heads, count, BLK) + array.shape[2:])

    query, keys, values, fading_exponent, beta = (
        split(a) for a in (query, keys, values, fading_exponent, beta)
    )
    summed = jnp.cumsum(fading_exponent, axis=-1)
    places = jnp.arange(BLK)
    inclusive = places[:, None] >= places[None, :]
    strict = places[:, None] > places[None, :]
    decay = jnp.exp(jnp.where(inclusive, summed[..., :, None] - summed[..., None, :], -1e30))
    k_beta = keys * beta[..., None]
    a_mat = jnp.where(
        strict, jnp.einsum("hncd,hnsd->hncs", k_beta, keys, precision=HIGH) * decay, 0.0
    )
    eye = jnp.eye(BLK, dtype=jnp.float32)
    t_mat = lax.linalg.triangular_solve(
        eye + a_mat,
        jnp.broadcast_to(eye, a_mat.shape),
        left_side=True,
        lower=True,
        unit_diagonal=True,
    )
    u_part = jnp.einsum("hncs,hnsd->hncd", t_mat, values * beta[..., None], precision=HIGH)
    w_part = jnp.einsum(
        "hncs,hnsd->hncd", t_mat, k_beta * jnp.exp(summed)[..., None], precision=HIGH
    )
    attend = jnp.where(
        inclusive, jnp.einsum("hncd,hnsd->hncs", query, keys, precision=HIGH) * decay, 0.0
    )
    q_dec = query * jnp.exp(summed)[..., None]
    k_dec = keys * jnp.exp(summed[..., -1:] - summed)[..., None]
    g_last = jnp.exp(summed[..., -1])
    return (u_part, w_part, q_dec, k_dec, attend, g_last)


def matmul_heads(left, right):
    return jnp.einsum("hij,hjk->hik", left, right, precision=HIGH)


def on_device(
    layer_input_sequence,
    probe_projection_matrix,
    address_projection_matrix,
    content_projection_matrix,
    result_valve_matrix,
    shrink_strength_matrix,
    causal_filter_coefficients,
    channel_group_fading_speed,
    summed_shrink_logs,
    result_scaling_vector,
    generated_probe_vector,
):
    tok_rows = layer_input_sequence.shape[0]
    local_width = probe_projection_matrix.shape[1]
    head_count = local_width // DK
    prompt_length = tok_rows * lax.axis_size("sp")
    piece = gathered_copies(layer_input_sequence, "tp", 1)
    columns = [
        m
        for m in (
            probe_projection_matrix,
            address_projection_matrix,
            content_projection_matrix,
            result_valve_matrix,
        )
    ]
    projected = jnp.stack([jnp.dot(piece, c, preferred_element_type=jnp.float32) for c in columns])
    rate_terms = jnp.einsum(
        "sd,rdh->srh", piece, shrink_strength_matrix, preferred_element_type=jnp.float32
    )
    projected, rate_terms = (projected, rate_terms)
    raw = projected.astype(jnp.bfloat16)
    rim = shifted(raw[:3, tok_rows - (CONV - 1) :], "sp", 1)
    extended = jnp.concatenate([rim, raw[:3]], axis=1).astype(jnp.float32)
    taps = causal_filter_coefficients.astype(jnp.float32)
    summed_taps = jnp.zeros((3, tok_rows, local_width), jnp.float32)
    for lag in range(CONV):
        summed_taps = summed_taps + taps[:, lag, None, :] * extended[:, lag : lag + tok_rows]
    convolved = silu(summed_taps)
    query = l2_unit(convolved[0].reshape(tok_rows, head_count, DK)) * DK ** (-0.5)
    keys = l2_unit(convolved[1].reshape(tok_rows, head_count, DK))
    values = convolved[2].reshape(tok_rows, head_count, DK)
    first_head = lax.axis_index("tp") * head_count
    diagonal_speed_entries = lax.dynamic_slice_in_dim(rate_terms, first_head, head_count, 2)
    diagonal_fading_multiplier = lax.dynamic_slice_in_dim(
        channel_group_fading_speed, first_head, head_count, 0
    )
    write_shift = math.log(4.0 * prompt_length / DK)
    beta = jax.nn.sigmoid(diagonal_speed_entries[:, 1, :] - write_shift)
    fading_exponent = (
        -diagonal_fading_multiplier[None, :] * jax.nn.softplus(diagonal_speed_entries[:, 0, :])
        + summed_shrink_logs
    )
    terms = block_terms(
        query.transpose(1, 0, 2),
        keys.transpose(1, 0, 2),
        values.transpose(1, 0, 2),
        fading_exponent.T,
        beta.T,
    )
    eye_heads = jnp.broadcast_to(jnp.eye(DK, dtype=jnp.float32), (head_count, DK, DK))
    zero_heads = jnp.zeros((head_count, DK, DK), jnp.float32)

    def local_step(carry, inputs):
        power, offset_state = carry
        u_i, w_i, qd_i, kd_i, a_i, gl_i = inputs
        w_power = jnp.einsum("hcd,hde->hce", w_i, power, precision=HIGH)
        v_zero = u_i - jnp.einsum("hcd,hde->hce", w_i, offset_state, precision=HIGH)
        base = jnp.einsum("hcd,hde->hce", qd_i, offset_state, precision=HIGH) + jnp.einsum(
            "hcs,hse->hce", a_i, v_zero, precision=HIGH
        )
        coupling = jnp.einsum("hcd,hde->hce", qd_i, power, precision=HIGH) - jnp.einsum(
            "hcs,hse->hce", a_i, w_power, precision=HIGH
        )
        power = power * gl_i[:, None, None] - jnp.einsum(
            "hcd,hce->hde", kd_i, w_power, precision=HIGH
        )
        offset_state = offset_state * gl_i[:, None, None] + jnp.einsum(
            "hcd,hce->hde", kd_i, v_zero, precision=HIGH
        )
        return ((power, offset_state), (base, coupling))

    inputs = tuple((jnp.moveaxis(t, 1, 0) for t in terms))
    (power, own_state), (base, coupling) = lax.scan(local_step, (eye_heads, zero_heads), inputs)
    packed = jnp.concatenate([power, own_state], axis=2)[None]
    every_piece = lax.all_gather(packed, "sp", axis=0, tiled=True)

    def walk(carry, piece):
        following = matmul_heads(piece[:, :, :DK], carry) + piece[:, :, DK:]
        return (following, carry)

    final_state, before = lax.scan(walk, zero_heads, every_piece)
    entry_state = lax.dynamic_index_in_dim(before, lax.axis_index("sp"), 0, keepdims=False)
    cache = final_state.astype(jnp.bfloat16)
    outputs = base + jnp.einsum("nhcd,hde->nhce", coupling, entry_state, precision=HIGH)
    heads_out = outputs.transpose(1, 0, 2, 3).reshape(head_count, tok_rows, DK).transpose(1, 0, 2)
    normed = heads_out * lax.rsqrt(jnp.mean(heads_out * heads_out, axis=-1, keepdims=True) + EPS)
    gate_rows = raw[3].reshape(tok_rows, head_count, DK).astype(jnp.float32)
    gated = normed * result_scaling_vector.astype(jnp.float32) * silu(gate_rows)
    mixed = gated.reshape(tok_rows, local_width).astype(jnp.bfloat16)
    unit_query = l2_unit(generated_probe_vector.astype(jnp.float32)) * DK ** (-0.5)
    new_read = jnp.einsum("nhd,hde->nhe", unit_query, cache.astype(jnp.float32), precision=HIGH)
    return (mixed, cache, new_read)


def solution(mesh):
    in_specs = (
        P("sp", "tp"),
        P(None, "tp"),
        P(None, "tp"),
        P(None, "tp"),
        P(None, "tp"),
        P(),
        P(None, None, "tp"),
        P(),
        P("sp", "tp"),
        P(),
        P("sp", "tp", None),
    )
    out_specs = (P("sp", "tp"), P("tp", None, None), P("sp", "tp", None))
    return jax.shard_map(
        on_device, mesh=mesh, in_specs=in_specs, out_specs=out_specs, check_vma=False
    )
```

profile of v0, /device:TPU:2, one launch (start us, length us, event | category | flops | bytes accessed | tf_op | source)
XLA Modules:
  0.0 394.5 jit_solution(7289248820536227078)
XLA Ops:
  7.2 2.3 broadcast_in_dim.65
  9.4 9.5 %all-to-all-start = ((bf16[8,384,256]{2,1,0:T(8,128)(2,1)}), bf16[8,384,256]{2,1,0:T(8,128)(2,1)S(1)}, u32[]{:S(2)}, u32[]{:S(2)}) async-start(bf16[8,384,256]{2,1,0:T(8,128)(2,1)} %broadcast_in_dim.65), calls=%async_computation | async-start | bytes 3145728 | tf_op jit(solution)/shard_map/all_to_all | solution.py:16
  20.4 18.7 %all-to-all-done = bf16[8,384,256]{2,1,0:T(8,128)(2,1)S(1)} async-done(((bf16[8,384,256]{2,1,0:T(8,128)(2,1)}), bf16[8,384,256]{2,1,0:T(8,128)(2,1)S(1)}, u32[]{:S(2)}, u32[]{:S(2)}) %all-to-all-start) | async-done | bytes 1572896 | tf_op jit(solution)/shard_map/all_to_all | solution.py:16
  39.1 1.2 copy-done.1
  40.2 1.6 copy.42
  44.5 1.3 collective-permute-start
  48.5 29.5 %custom-call.3 = f32[1,6,1,64,64]{3,4,2,1,0:T(8,128)S(1)} custom-call(f32[1,6,1,64,64]{4,3,2,1,0:T(8,128)S(1)} %fusion.57), custom_call_target="InvertDiagBlocksLowerTriangular" | custom-call | tf_op jit(solution)/shard_map/triangular_solve | solution.py:66
  80.4 28.9 %while.30 = (s32[]{:T(128)}, f32[1,128,128]{2,1,0:T(8,128)S(1)}, f32[1,128,128]{2,1,0:T(8,128)S(1)}, f32[6,1,64,128]{3,2,1,0:T(8,128)}, f32[6,1,64,128]{3,2,1,0:...) while((s32[]{:T(128)}, f32[1,128,128]{2,1,0:T(8,128)S(1)}, ...), condition=%wide.region_4.5_spmd.clone, body=%wide.region_3.4_spmd.clone.sunk | while | flops 88219648 | bytes 1215665 | solution.py:174
  83.3 0.9 fusion.168
  84.2 1.0 fusion.167
  88.1 0.9 fusion.168
  89.0 1.0 fusion.167
  92.9 0.9 fusion.168
  93.9 1.0 fusion.167
  97.7 0.9 fusion.168
  98.7 1.0 fusion.167
  102.6 0.9 fusion.168
  103.5 1.0 fusion.167
  107.4 0.9 fusion.168
  108.3 1.0 fusion.167
  111.3 157.5 %all-gather.3.cloned.1.call-done = f32[64,128,256]{2,1,0:T(8,128)} async-done(((f32[1,128,256]{2,1,0:T(8,128)}), f32[64,128,256]{2,1,0:T(8,128)}) %all-gather.3.cloned.1.call-update) | async-done | bytes 8388624 | tf_op jit(solution)/shard_map/all_gather | solution.py:176
  268.8 114.5 %while.31 = (s32[]{:T(128)}, f32[1,128,128]{2,1,0:T(8,128)S(1)}, f32[64,1,128,128]{3,2,1,0:T(8,128)}, f32[64,1,128,256]{3,2,1,0:T(8,128)}, s32[]{:T(128)}, /*index=5*/s32[]{:T(128)}) while((s32[]{:T(128)}, f32[1,128,128]{2,1,0:T(8,128)S(1)}, f32[64,1,128,128]{3,2,1,0:T(8,128)}, f32[64,1,128,256]{3,2,1,0:T(8,128)}, s32[]{:T(128)}, ...), condition=%wide.region_6.7_spmd.clone, body=%wide.region_5.6_spmd.clone.sunk | while | flops 25214980 | bytes 787028 | solution.py:182
  383.4 1.2 multiply_reduce_fusion
  385.4 2.3 fusion.69
  (373 shorter events, 139.8 us)
Async XLA Ops:
  7.2 34.7 %copy-start = (bf16[2048,128]{1,0:T(8,128)(2,1)S(1)}, bf16[2048,128]{1,0:T(8,128)(2,1)}, u32[]{:S(2)}) copy-start(bf16[2048,128]{1,0:T(8,128)(2,1)} %param.16) | copy-start | bytes 1572868
  9.4 9.5 %copy-start.11 = (f32[8]{0:T(128)S(1)}, f32[8]{0:T(128)}, u32[]{:S(2)}) copy-start(f32[8]{0:T(128)} %param.22) | copy-start | bytes 100
  9.4 10.8 %copy-start.8 = (bf16[3,4,128]{2,1,0:T(4,128)(2,1)S(1)}, bf16[3,4,128]{2,1,0:T(4,128)(2,1)}, u32[]{:S(2)}) copy-start(bf16[3,4,128]{2,1,0:T(4,128)(2,1)} %param.21) | copy-start | bytes 9220
  9.4 29.6 %all-to-all-start = ((bf16[8,384,256]{2,1,0:T(8,128)(2,1)}), bf16[8,384,256]{2,1,0:T(8,128)(2,1)S(1)}, u32[]{:S(2)}, u32[]{:S(2)}) async-start(bf16[8,384,256]{2,1,0:T(8,128)(2,1)} %broadcast_in_dim.65), calls=%async_computation | async-start | bytes 3145728 | tf_op jit(solution)/shard_map/all_to_all | solution.py:16
  18.9 249.9 %all-gather.3.cloned.1.call-start = ((), (), s32[]{:S(2)}) async-start(), calls=%async_computation.1 | async-start | bytes 8519680 | tf_op jit(solution)/shard_map/all_gather | solution.py:176
  39.1 1.2 copy-start.1
  41.8 1.0 copy-start.2
  42.9 1.0 copy-start.3
  43.9 1.9 copy-start.7
  43.9 2.4 copy-start.9
  44.5 2.6 collective-permute-start
  80.4 29.7 %copy-start.12 = (bf16[128]{0:T(256)(128)(2,1)S(1)}, bf16[128]{0:T(256)(128)(2,1)}, u32[]{:S(2)}) copy-start(bf16[128]{0:T(256)(128)(2,1)} %param.24) | copy-start | bytes 772
  80.4 29.7 %copy-start.10 = (bf16[1,1,128]{2,1,0:T(2,128)(2,1)S(1)}, bf16[1,1,128]{2,1,0:T(2,128)(2,1)}, u32[]{:S(2)}) copy-start(bf16[1,1,128]{2,1,0:T(2,128)(2,1)} %param.25) | copy-start | bytes 772
  268.8 114.5 %copy-start.4 = (f32[6,1,64,128]{3,2,1,0:T(8,128)S(1)}, f32[6,1,64,128]{3,2,1,0:T(8,128)}, u32[]{:S(2)}) copy-start(f32[6,1,64,128]{3,2,1,0:T(8,128)} %get-tuple-element.86) | copy-start | bytes 589828
  268.8 114.6 %copy-start.5 = (f32[6,1,64,128]{3,2,1,0:T(8,128)S(1)}, f32[6,1,64,128]{3,2,1,0:T(8,128)}, u32[]{:S(2)}) copy-start(f32[6,1,64,128]{3,2,1,0:T(8,128)} %get-tuple-element.90) | copy-start | bytes 589828
  384.7 2.9 copy-start.6
Sparse Core Ops, SparseCore 0:
  110.1 158.6 all-gather.2
where the time goes:
time: 396 us; the launch traced here: 394 us
  waiting for transfers between devices  176 us (44%)
  other arithmetic  72.4 us (18%)
  local copies, waits for them, and re-layouts  69.4 us (18%)
  matrix products  47.2 us (12%)
  between operations  15.7 us (4%)
  starting transfers between devices  10.8 us (3%)
    all_gather x1, waiting for transfers between devices, on_device(): every_piece = lax.all_gather(packed, 'sp', axis=0, tiled=True)  157 us
    squeeze x64, local copies, waits for them, and re-layouts, on_device(): final_state, before = lax.scan(walk, zero_heads, every_piece)  58.4 us
    dynamic_update_slice x64, other arithmetic, on_device(): final_state, before = lax.scan(walk, zero_heads, every_piece)  40.2 us
    another operation x4, other arithmetic, block_terms(): lax.linalg.triangular_solve(eye + a_mat, jnp.broadcast_to(eye, a_mat.shap...  29.6 us
    all_to_all x1, waiting for transfers between devices, sent_to_all(): lax.all_to_all(jnp.broadcast_to(shard[None], (count, *shard.shape)), axis...  18.7 us
    dot_general x64, matrix products, matmul_heads(): return jnp.einsum('hij,hjk->hik', left, right, precision=HIGH)  13.2 us
    all_to_all x1, starting transfers between devices, sent_to_all(): lax.all_to_all(jnp.broadcast_to(shard[None], (count, *shard.shape)), axis...  9.5 us
  transfers between devices with their start and end apart: 3, of which 2 were waited for; matrix products, arithmetic and copies ran while one was open for 1% of the time, Pallas kernels for 0%

commit v1 on v0

--- a/solution.py
+++ b/solution.py
@@ -173,7 +173,15 @@
     inputs = tuple((jnp.moveaxis(t, 1, 0) for t in terms))
     (power, own_state), (base, coupling) = lax.scan(local_step, (eye_heads, zero_heads), inputs)
     packed = jnp.concatenate([power, own_state], axis=2)[None]
-    every_piece = lax.all_gather(packed, "sp", axis=0, tiled=True)
+    every_piece = jnp.concatenate(
+        lax.all_to_all(
+            jnp.stack([packed for _ in range(lax.axis_size("sp"))], axis=0),
+            axis_name="sp",
+            split_axis=0,
+            concat_axis=0,
+        ),
+        axis=0,
+    )
 
     def walk(carry, piece):
         following = matmul_heads(piece[:, :, :DK], carry) + piece[:, :, DK:]

time: 396 us -> 614 us (1.55)
  the two profiles are of different devices: /device:TPU:2 before, /device:TPU:8 now
where the time goes in v1:
time: 614 us; the launch traced here: 612 us
  waiting for transfers between devices  390 us (64%)
  local copies, waits for them, and re-layouts  73.7 us (12%)
  other arithmetic  71.8 us (12%)
  matrix products  46.2 us (8%)
  starting transfers between devices  25.3 us (4%)
    all_to_all x1, waiting for transfers between devices, on_device(): lax.all_to_all(jnp.stack([packed for _ in range(lax.axis_size('sp'))], ax...  367 us
    squeeze x64, local copies, waits for them, and re-layouts, on_device(): final_state, before = lax.scan(walk, zero_heads, every_piece)  58.4 us
    dynamic_update_slice x64, other arithmetic, on_device(): final_state, before = lax.scan(walk, zero_heads, every_piece)  40.3 us
    another operation x4, other arithmetic, block_terms(): lax.linalg.triangular_solve(eye + a_mat, jnp.broadcast_to(eye, a_mat.shap...  29.6 us
    all_to_all x1, waiting for transfers between devices, sent_to_all(): lax.all_to_all(jnp.broadcast_to(shard[None], (count, *shard.shape)), axis...  20.1 us
    all_to_all x1, starting transfers between devices, on_device(): lax.all_to_all(jnp.stack([packed for _ in range(lax.axis_size('sp'))], ax...  17.4 us
    dot_general x64, matrix products, matmul_heads(): return jnp.einsum('hij,hjk->hik', left, right, precision=HIGH)  13.2 us
  transfers between devices with their start and end apart: 3, of which 3 were waited for; matrix products, arithmetic and copies ran while one was open for 0% of the time, Pallas kernels for 0%

profile of v1, /device:TPU:8, one launch (start us, length us, event | category | flops | bytes accessed | tf_op | source)
XLA Modules:
  0.0 612.1 jit_solution(17528359774922078529)
XLA Ops:
  0.6 2.3 broadcast_in_dim.62
  2.9 4.4 all-to-all-start
  8.8 20.1 %all-to-all-done = bf16[8,384,256]{2,1,0:T(8,128)(2,1)S(1)} async-done(((bf16[8,384,256]{2,1,0:T(8,128)(2,1)}), bf16[8,384,256]{2,1,0:T(8,128)(2,1)S(1)}, u32[]{:S(2)}, u32[]{:S(2)}) %all-to-all-start) | async-done | bytes 1572896 | tf_op jit(solution)/shard_map/all_to_all | solution.py:16
  28.9 1.2 copy-done.1
  30.1 1.6 copy.42
  34.4 3.5 collective-permute-start
  39.1 3.1 collective-permute-done
  43.6 29.5 %custom-call.3 = f32[1,6,1,64,64]{3,4,2,1,0:T(8,128)S(1)} custom-call(f32[1,6,1,64,64]{4,3,2,1,0:T(8,128)S(1)} %fusion.57), custom_call_target="InvertDiagBlocksLowerTriangular" | custom-call | tf_op jit(solution)/shard_map/triangular_solve | solution.py:66
  75.4 28.9 %while.30 = (s32[]{:T(128)}, f32[1,128,128]{2,1,0:T(8,128)S(1)}, f32[1,128,128]{2,1,0:T(8,128)S(1)}, f32[6,1,64,128]{3,2,1,0:T(8,128)}, f32[6,1,64,128]{3,2,1,0:...) while((s32[]{:T(128)}, f32[1,128,128]{2,1,0:T(8,128)S(1)}, ...), condition=%wide.region_4.5_spmd.clone, body=%wide.region_3.4_spmd.clone.sunk | while | flops 88219648 | bytes 1215665 | solution.py:174
  78.3 0.9 fusion.168
  79.3 1.0 fusion.167
  83.2 0.9 fusion.168
  84.1 1.0 fusion.167
  88.0 0.9 fusion.168
  88.9 1.0 fusion.167
  93.7 1.0 fusion.167
  98.5 1.0 fusion.167
  103.4 1.0 fusion.167
  104.3 4.2 stack.25
  108.6 17.4 %all-to-all-start.1 = ((f32[64,1,1,128,256]{4,3,2,1,0:T(8,128)}), f32[64,1,1,128,256]{4,3,2,1,0:T(8,128)}, u32[]{:S(2)}, u32[]{:S(2)}) async-start(f32[64,1,1,128,256]{4,3,2,1,0:T(8,128)} %stack.25), calls=%async_computation.1 | async-start | bytes 16777216 | tf_op jit(solution)/shard_map/all_to_all | solution.py:177
  127.3 366.9 %all-to-all-done.1 = f32[64,1,1,128,256]{4,3,2,1,0:T(8,128)} async-done(((f32[64,1,1,128,256]{4,3,2,1,0:T(8,128)}), f32[64,1,1,128,256]{4,3,2,1,0:T(8,128)}, u32[]{:S(2)}, u32[]{:S(2)}) %all-to-all-start.1) | async-done | bytes 8388640 | tf_op jit(solution)/shard_map/all_to_all | solution.py:177
  494.2 114.6 %while.31 = (s32[]{:T(128)}, f32[1,128,128]{2,1,0:T(8,128)S(1)}, f32[64,1,128,128]{3,2,1,0:T(8,128)}, f32[64,1,128,256]{3,2,1,0:T(8,128)}, s32[]{:T(128)}, /*index=5*/s32[]{:T(128)}) while((s32[]{:T(128)}, f32[1,128,128]{2,1,0:T(8,128)S(1)}, f32[64,1,128,128]{3,2,1,0:T(8,128)}, f32[64,1,128,256]{3,2,1,0:T(8,128)}, s32[]{:T(128)}, ...), condition=%wide.region_6.7_spmd.clone, body=%wide.region_5.6_spmd.clone.sunk | while | flops 25214980 | bytes 787028 | solution.py:190
  608.9 1.2 multiply_reduce_fusion
  610.9 1.2 fusion.69
  (375 shorter events, 142.0 us)
Async XLA Ops:
  0.6 31.0 %copy-start = (bf16[2048,128]{1,0:T(8,128)(2,1)S(1)}, bf16[2048,128]{1,0:T(8,128)(2,1)}, u32[]{:S(2)}) copy-start(bf16[2048,128]{1,0:T(8,128)(2,1)} %param.16) | copy-start | bytes 1572868
  2.9 4.5 copy-start.12
  2.9 5.8 copy-start.8
  2.9 26.0 %all-to-all-start = ((bf16[8,384,256]{2,1,0:T(8,128)(2,1)}), bf16[8,384,256]{2,1,0:T(8,128)(2,1)S(1)}, u32[]{:S(2)}, u32[]{:S(2)}) async-start(bf16[8,384,256]{2,1,0:T(8,128)(2,1)} %broadcast_in_dim.62), calls=%async_computation | async-start | bytes 3145728 | tf_op jit(solution)/shard_map/all_to_all | solution.py:16
  28.9 1.2 copy-start.1
  31.7 1.0 copy-start.2
  32.7 1.0 copy-start.3
  33.8 4.1 copy-start.7
  33.8 4.6 copy-start.9
  34.4 7.9 %collective-permute-start = (bf16[3,3,128]{2,1,0:T(4,128)(2,1)S(1)}, bf16[3,3,128]{2,1,0:T(4,128)(2,1)S(1)}, u32[]{:S(2)}, u32[]{:S(2)}) collective-permute-start(bf16[3,3,128]{2,1,0:T(4,128)(2,1)S(1)} %pad_maximum_fusion), channel_id=1, source_target_pairs={{0,8},{8,16},{16,24},{24,32},{32,40},{40,48},{48,56},{56,64},{64,7... | collective-permute-start | bytes 6920 | tf_op jit(solution)/shard_map/ppermute | solution.py:35
  108.6 17.4 %copy-start.13 = (bf16[128]{0:T(256)(128)(2,1)S(1)}, bf16[128]{0:T(256)(128)(2,1)}, u32[]{:S(2)}) copy-start(bf16[128]{0:T(256)(128)(2,1)} %param.24) | copy-start | bytes 772
  108.6 17.4 %copy-start.10 = (bf16[1,1,128]{2,1,0:T(2,128)(2,1)S(1)}, bf16[1,1,128]{2,1,0:T(2,128)(2,1)}, u32[]{:S(2)}) copy-start(bf16[1,1,128]{2,1,0:T(2,128)(2,1)} %param.25) | copy-start | bytes 772
  108.6 385.7 %all-to-all-start.1 = ((f32[64,1,1,128,256]{4,3,2,1,0:T(8,128)}), f32[64,1,1,128,256]{4,3,2,1,0:T(8,128)}, u32[]{:S(2)}, u32[]{:S(2)}) async-start(f32[64,1,1,128,256]{4,3,2,1,0:T(8,128)} %stack.25), calls=%async_computation.1 | async-start | bytes 16777216 | tf_op jit(solution)/shard_map/all_to_all | solution.py:177
  494.2 114.6 %copy-start.4 = (f32[6,1,64,128]{3,2,1,0:T(8,128)S(1)}, f32[6,1,64,128]{3,2,1,0:T(8,128)}, u32[]{:S(2)}) copy-start(f32[6,1,64,128]{3,2,1,0:T(8,128)} %get-tuple-element.86) | copy-start | bytes 589828
  494.2 114.6 %copy-start.5 = (f32[6,1,64,128]{3,2,1,0:T(8,128)S(1)}, f32[6,1,64,128]{3,2,1,0:T(8,128)}, u32[]{:S(2)}) copy-start(f32[6,1,64,128]{3,2,1,0:T(8,128)} %get-tuple-element.90) | copy-start | bytes 589828
  494.2 116.6 %copy-start.11 = (bf16[2048,128]{1,0:T(8,128)(2,1)S(1)}, bf16[2048,128]{1,0:T(8,128)(2,1)}, u32[]{:S(2)}) copy-start(bf16[2048,128]{1,0:T(8,128)(2,1)} %param.19) | copy-start | bytes 1572868
  610.2 1.9 copy-start.6
